TPU v7x, 128 devices: a whole 4x4x4 slice. The times are simulated.
128 devices in a mesh: sp: 32 (over z, y, core), tp: 4 (over x).
Axes of the slice: x: 4, y: 4, z: 4, core: 2. Of those that a mesh axis runs over, the one named last changes fastest.
Arguments:
- query_rows: bfloat16 [32768, 1024], P('sp', 'tp'), may hold values from -6 to 6
- key_rows: bfloat16 [32768, 1024], P('sp', 'tp'), may hold values from -6 to 6
- value_rows: bfloat16 [32768, 1024], P('sp', 'tp'), may hold values from -6 to 6
- input_gate: float32 [8, 32768], P('tp', 'sp'), may hold values from -4 to 255
- forget_gate: float32 [8, 32768], P('tp', 'sp'), may hold values from -3 to 20
- output_gate: bfloat16 [32768, 1024], P('sp', 'tp'), may hold values from -6 to 6
- documents: int32 [32768], P('sp'), may hold values from 0 to 7, never falling along the last dimension, each value on 1 to 6144 neighbouring positions
- residual: bfloat16 [32768, 2048], P(('sp', 'tp')), may hold values from -6 to 6
- out_weight: bfloat16 [1024, 2048], P('tp'), may hold values from -0.375 to 0.375
- norm_gain: bfloat16 [2048], replicated, may hold values from 0.099609375 to 1.8984375
- gate_weight: bfloat16 [2048, 5632], P('sp', 'tp'), may hold values from -0.125 to 0.125
- up_weight: bfloat16 [2048, 5632], P('sp', 'tp'), may hold values from -0.125 to 0.125
- down_weight: bfloat16 [5632, 2048], P('tp', 'sp'), may hold values from -0.15625 to 0.15625
Outputs:
- layer_out: bfloat16 [32768, 2048], P(('sp', 'tp'))
Inputs may be any that keep to these rules, and one draw needn't show every extreme that they name: `documents`: document numbers never fall along the positions; each document covers 1 to 6144 positions and one covers exactly 6144.
All inputs are finite; a program needn't handle non-finite values.
Results may differ from a plain program's by a relative error of at most 0.013.
Values may be sent and summed in bfloat16 or wider, within the bound.
A program may use at most 128 MiB of HBM per device.

v0:
```python
import jax
import jax.numpy as jnp
from jax import lax
from jax.sharding import Mesh
from jax.sharding import PartitionSpec as P

HD = 128
BLOCK = 128
SP = ("sp_0", "sp_1", "sp_2")
SP_TP = ("sp_0", "sp_1", "sp_2", "tp")
neg_large = -1e30
norm_eps = 1e-06
highest = lax.Precision.HIGHEST


def gather_turned(arrays, axis, dims):
    turned = [jnp.moveaxis(a, dim, 0) for a, dim in zip(arrays, dims)]
    both = jnp.concatenate([t.reshape(len(t), -1) for t in turned], axis=1)
    whole, at, finished = (lax.all_gather(both, axis, axis=0, tiled=True), 0, [])
    for t, dim in zip(turned, dims):
        slab = whole[:, at : at + t[0].size].reshape(-1, *t.shape[1:])
        finished.append(jnp.moveaxis(slab, 0, dim))
        at += t[0].size
    return tuple(finished)


def nothing_yet(array, identity):
    return jax.tree.map(
        lambda part, zero: jnp.zeros_like(part) + jnp.asarray(zero, part.dtype), array, identity
    )


def all_in_one(array, axis):
    leaves = jax.tree.leaves(array)
    sequence = sorted(range(len(leaves)), key=lambda k: -leaves[k].size)
    width = (1, *leaves[sequence[0]].shape)[-1]
    lines = [
        jnp.pad(leaves[k].reshape(-1), (0, -leaves[k].size % width)).reshape(-1, width)
        for k in sequence
    ]
    both, at, found = (lax.all_gather(jnp.concatenate(lines), axis), 0, {})
    for k, line in zip(sequence, lines):
        slab = both[:, at : at + len(line)].reshape(len(both), -1)
        found[k] = slab[:, : leaves[k].size].reshape(-1, *leaves[k].shape)
        at += len(line)
    numbers = iter(range(len(leaves)))
    return jax.tree.map(lambda _: found[next(numbers)], array)


def gathered_by_type(array, axis):
    leaves, found = (jax.tree.leaves(array), {})
    for leading, a in enumerate(leaves):
        if leading not in found:
            alike = [k for k, b in enumerate(leaves) if b.dtype == a.dtype]
            got = (
                all_in_one([leaves[k] for k in alike], axis)
                if len(alike) > 1
                else [lax.all_gather(a, axis)]
            )
            for k, b in zip(alike, got):
                found[k] = b
    numbers = iter(range(len(leaves)))
    return jax.tree.map(lambda _: found[next(numbers)], array)


def prefix_by_axis(array, axes, combine, identity):
    before = start = nothing_yet(array, identity)
    total = array
    for axis in reversed(axes):
        devices, position = (lax.axis_size(axis), lax.axis_index(axis))
        pieces = gathered_by_type(total, axis)
        inside, total = (start, start)
        for k in range(devices):
            passed = k < position
            total = combine(total, jax.tree.map(lambda part: part[k], pieces))
            inside = jax.tree.map(lambda new, old: jnp.where(passed, new, old), total, inside)
        before = combine(inside, before)
    return before


def block_step(carried, inputs):
    memory, normer, stab_prev, carry_doc = carried
    queries, key_float, value_float, gate_in, log_forget, docs = inputs
    cumlog = jnp.cumsum(log_forget, axis=1)
    length = docs.shape[0]
    target_positions = jnp.arange(length)
    same_doc = (docs[:, None] == docs[None, :]) & (
        target_positions[:, None] >= target_positions[None, :]
    )
    log_weight = jnp.where(
        same_doc[None], cumlog[:, :, None] - cumlog[:, None, :] + gate_in[:, None, :], neg_large
    )
    carried_log = jnp.where((docs == carry_doc)[None, :], cumlog + stab_prev[:, None], neg_large)
    stabilizer = jnp.maximum(carried_log, jnp.max(log_weight, axis=2))
    scores = jnp.einsum("lhd,shd->hls", queries, key_float, precision=highest)
    weighted = scores * jnp.exp(log_weight - stabilizer[:, :, None])
    carried_scale = jnp.exp(carried_log - stabilizer)
    numerator = carried_scale[:, :, None] * jnp.einsum(
        "lhd,hde->hle", queries, memory, precision=highest
    )
    numerator = numerator + jnp.einsum("hls,she->hle", weighted, value_float, precision=highest)
    denominator = carried_scale * jnp.einsum(
        "lhd,hd->hl", queries, normer, precision=highest
    ) + jnp.sum(weighted, axis=2)
    outputs = numerator / jnp.maximum(jnp.abs(denominator), 1.0)[:, :, None]
    last_doc = docs[-1]
    inject_log = jnp.where(
        (docs == last_doc)[None, :], cumlog[:, -1:] - cumlog + gate_in, neg_large
    )
    inject_max = jnp.max(inject_log, axis=1)
    weights = jnp.exp(inject_log - inject_max[:, None])
    continues = carry_doc == last_doc
    stab_new = jnp.where(continues, jnp.maximum(cumlog[:, -1] + stab_prev, inject_max), inject_max)
    decay_scale = jnp.where(continues, jnp.exp(cumlog[:, -1] + stab_prev - stab_new), 0.0)
    inject = jnp.exp(inject_max - stab_new)
    memory_step = jnp.einsum(
        "lhd,lhe->hde", key_float * weights.T[:, :, None], value_float, precision=highest
    )
    normer_step = jnp.einsum("hl,lhd->hd", weights, key_float, precision=highest)
    memory = decay_scale[:, None, None] * memory + inject[:, None, None] * memory_step
    normer = decay_scale[:, None] * normer + inject[:, None] * normer_step
    return ((memory, normer, stab_new, last_doc), jnp.transpose(outputs, (1, 0, 2)))


def run_blocks(queries, key_float, value_float, gate_in, log_forget, docs, start_state):
    length, heads, width = queries.shape
    count = length // BLOCK
    inputs = (
        queries.reshape(count, BLOCK, heads, width),
        key_float.reshape(count, BLOCK, heads, width),
        value_float.reshape(count, BLOCK, heads, width),
        jnp.moveaxis(gate_in.reshape(heads, count, BLOCK), 1, 0),
        jnp.moveaxis(log_forget.reshape(heads, count, BLOCK), 1, 0),
        docs.reshape(count, BLOCK),
    )
    final, outputs = lax.scan(block_step, start_state, inputs)
    return (outputs.reshape(length, heads, width), final)


def join_states(earlier, later_part):
    memory_early, normer_early, stab_early, total_early, doc_early = earlier
    memory_late, normer_late, stab_late, total_late, doc_late = later_part
    continues = doc_late == doc_early
    is_empty = doc_late < 0
    stab_both = jnp.where(continues, jnp.maximum(total_late + stab_early, stab_late), stab_late)
    scale_early = jnp.where(continues, jnp.exp(total_late + stab_early - stab_both), 0.0)
    scale_late = jnp.exp(stab_late - stab_both)
    memory = scale_early[:, None, None] * memory_early + scale_late[:, None, None] * memory_late
    normer = scale_early[:, None] * normer_early + scale_late[:, None] * normer_late
    return (
        jnp.where(is_empty, memory_early, memory),
        jnp.where(is_empty, normer_early, normer),
        jnp.where(is_empty, stab_early, stab_both),
        total_early + total_late,
        jnp.where(is_empty, doc_early, doc_late),
    )


def body(
    query_rows,
    key_rows,
    value_rows,
    input_gate,
    forget_gate,
    output_gate,
    documents,
    residual,
    out_weight,
    norm_gain,
    gate_weight,
    up_weight,
    down_weight,
):
    whole_gate, whole_up, whole_down = gather_turned(
        (gate_weight, up_weight, down_weight), SP, (0, 0, 1)
    )
    tokens = query_rows.shape[0]
    local_heads = input_gate.shape[0]
    queries = query_rows.astype(jnp.float32).reshape(tokens, local_heads, HD) * HD ** (-0.5)
    key_float = key_rows.astype(jnp.float32).reshape(tokens, local_heads, HD)
    value_float = value_rows.astype(jnp.float32).reshape(tokens, local_heads, HD)
    log_forget = jax.nn.log_sigmoid(forget_gate)
    cumlog = jnp.cumsum(log_forget, axis=1)
    total = cumlog[:, -1]
    last_doc = documents[-1]
    inject_log = jnp.where(
        (documents == last_doc)[None, :], total[:, None] - cumlog + input_gate, neg_large
    )
    inject_max = jnp.max(inject_log, axis=1)
    weights = jnp.exp(inject_log - inject_max[:, None])
    memory = jnp.einsum(
        "thd,the->hde", key_float * weights.T[:, :, None], value_float, precision=highest
    )
    normer = jnp.einsum("ht,thd->hd", weights, key_float, precision=highest)
    identity = (
        jnp.zeros_like(memory),
        jnp.zeros_like(normer),
        jnp.full_like(inject_max, neg_large),
        jnp.zeros_like(total),
        jnp.array(-1, jnp.int32),
    )
    before = prefix_by_axis(
        (memory, normer, inject_max, total, last_doc), SP, join_states, identity
    )
    cells, final = run_blocks(
        queries,
        key_float,
        value_float,
        input_gate,
        log_forget,
        documents,
        (before[0], before[1], before[2], before[4]),
    )
    gated = (cells.reshape(tokens, -1) * jax.nn.sigmoid(output_gate.astype(jnp.float32))).astype(
        jnp.bfloat16
    )
    mine = lax.all_to_all(gated, "tp", split_axis=0, concat_axis=1, tiled=True)
    projected = jnp.dot(
        mine,
        lax.all_gather(out_weight, "tp", axis=0, tiled=True),
        preferred_element_type=jnp.float32,
    )
    stream = residual.astype(jnp.float32) + projected
    normed = stream * lax.rsqrt(jnp.mean(stream * stream, axis=1, keepdims=True) + norm_eps)
    normed = (normed * norm_gain.astype(jnp.float32)).astype(jnp.bfloat16)
    rows_all = lax.all_gather(normed, "tp", axis=0, tiled=True)
    gate_act = jnp.dot(rows_all, whole_gate, preferred_element_type=jnp.float32)
    up_act = jnp.dot(rows_all, whole_up, preferred_element_type=jnp.float32)
    hidden = (jax.nn.silu(gate_act) * up_act).astype(jnp.bfloat16)
    partial_sum = jnp.dot(hidden, whole_down, preferred_element_type=jnp.float32)
    down = lax.psum_scatter(
        partial_sum.astype(jnp.bfloat16), "tp", scatter_dimension=0, tiled=True
    ).astype(jnp.float32)
    return (stream + 0.5 * down).astype(jnp.bfloat16)


def solution(mesh):
    torus = Mesh(mesh.devices.reshape(4, 4, 2, mesh.shape["tp"]), ("sp_0", "sp_1", "sp_2", "tp"))
    in_specs = (
        P(SP, "tp"),
        P(SP, "tp"),
        P(SP, "tp"),
        P("tp", SP),
        P("tp", SP),
        P(SP, "tp"),
        P(SP),
        P(SP_TP, None),
        P("tp", None),
        P(),
        P(SP, "tp"),
        P(SP, "tp"),
        P("tp", SP),
    )
    out_specs = P(SP_TP, None)
    return jax.shard_map(body, mesh=torus, in_specs=in_specs, out_specs=out_specs, check_vma=False)
```

profile of v0, /device:TPU:1, one launch (start us, length us, event | category | flops | bytes accessed | tf_op | source)
XLA Modules:
  0.0 448.9 jit_solution(14347902271754953552)
XLA Ops:
  8.7 1.2 dynamic-slice
  10.0 1.9 slice_dynamic-update-slice_fusion
  11.9 1.3 broadcast_compare_fusion
  14.4 0.9 fusion.108
  15.4 1.2 copy.56
  16.7 1.4 fusion.34
  18.0 1.7 fusion.32
  19.8 3.2 all-gather.3
  23.6 1.8 all-reduce.6
  31.0 11.8 %all-gather.4 = f32[4,260,128]{2,1,0:T(8,128)S(1)} all-gather(f32[1,260,128]{2,1,0:T(8,128)S(1)} %maximum_bitcast_fusion.1), channel_id=3, replica_groups=mesh['sp_0'=4,'sp_1'=4,'sp_2'=2,'tp'=4] {'sp_1'}, dimensions={0}, use_global_device_ids=true | all-gather | bytes 665600 | tf_op jit(solution)/shard_map/all_gather | solution.py:41
  42.8 0.8 fusion.113
  45.5 6.5 %all-reduce.7 = s32[4]{0:T(128)S(1)} all-reduce(s32[4]{0:T(128)S(1)} %dynamic-update-slice.1), channel_id=1, replica_groups=mesh['sp_0'=4,'sp_1'=4,'sp_2'=2,'tp'=4] {'sp_1'}, use_global_device_ids=true, to_apply=%add.7 | all-reduce | flops 4 | bytes 32
  61.6 11.7 %all-gather.5 = f32[4,260,128]{2,1,0:T(8,128)S(1)} all-gather(f32[1,260,128]{2,1,0:T(8,128)S(1)} %maximum_bitcast_fusion.2), channel_id=4, replica_groups=mesh['sp_0'=4,'sp_1'=4,'sp_2'=2,'tp'=4] {'sp_0'}, dimensions={0}, use_global_device_ids=true | all-gather | bytes 665600 | tf_op jit(solution)/shard_map/all_gather | solution.py:41
  74.2 1.5 reshape.2044
  75.6 1.2 dynamic-slice.2
  77.6 7.2 %all-reduce.8 = s32[4]{0:T(128)S(1)} all-reduce(s32[4]{0:T(128)S(1)} %dynamic-update-slice.2), channel_id=1, replica_groups=mesh['sp_0'=4,'sp_1'=4,'sp_2'=2,'tp'=4] {'sp_0'}, use_global_device_ids=true, to_apply=%add.8 | all-reduce | flops 4 | bytes 32
  92.9 1.1 convert_multiply_fusion
  94.1 1.5 reshape.2046
  95.9 1.8 add_select_fusion.3
  97.7 112.4 %while.18 = (s32[]{:T(128)}, f32[2,128,128]{2,1,0:T(8,128)S(1)}, f32[2,128]{1,0:T(2,128)S(1)}, f32[2]{0:T(128)S(1)}, s32[]{:T(128)}, /*index=5*/f32[8,128,2,128]...) while((s32[]{:T(128)}, f32[2,128,128]{2,1,0:T(8,128)S(1)}, ...), condition=%wide.region_8.9_spmd, body=%wide.region_3.8_spmd.sunk | while | flops 202756624 | bytes 3499011 | solution.py:136
  100.9 0.9 fusion.154
  102.2 0.9 constant_dynamic-slice_fusion.10
  103.3 0.9 constant_dynamic-slice_fusion.9
  106.4 4.7 %dynamic_update_slice.5 = f32[8,128,2,128]{1,0,3,2:T(8,128)} dynamic-update-slice(f32[8,128,2,128]{1,0,3,2:T(8,128)} %get-tuple-element.360, f32[1,128,2,128]{1,0,3,2:T(1,128)S(1)} %copy.134, s32[]{:T(128)S(6)} %copy.145, s32[]{:T(128)} %constant.31.clone.1..sunk, s32[]{:T(128)} %constant.31.clone.1..sunk, s32[]{:T(128)} %constant.31.clone.1..sunk) | dynamic-update-slice | bytes 262148 | tf_op jit(solution)/shard_map/while/body/jit(dynamic_update_index_in_dim)/dynamic_update_slice | solution.py:136
  114.9 0.9 fusion.154
  116.2 0.9 constant_dynamic-slice_fusion.10
  117.3 0.9 constant_dynamic-slice_fusion.9
  120.5 4.7 %dynamic_update_slice.5 = f32[8,128,2,128]{1,0,3,2:T(8,128)} dynamic-update-slice(f32[8,128,2,128]{1,0,3,2:T(8,128)} %get-tuple-element.360, f32[1,128,2,128]{1,0,3,2:T(1,128)S(1)} %copy.134, s32[]{:T(128)S(6)} %copy.145, s32[]{:T(128)} %constant.31.clone.1..sunk, s32[]{:T(128)} %constant.31.clone.1..sunk, s32[]{:T(128)} %constant.31.clone.1..sunk) | dynamic-update-slice | bytes 262148 | tf_op jit(solution)/shard_map/while/body/jit(dynamic_update_index_in_dim)/dynamic_update_slice | solution.py:136
  129.0 0.9 fusion.154
  130.2 0.9 constant_dynamic-slice_fusion.10
  131.4 0.9 constant_dynamic-slice_fusion.9
  134.5 4.7 %dynamic_update_slice.5 = f32[8,128,2,128]{1,0,3,2:T(8,128)} dynamic-update-slice(f32[8,128,2,128]{1,0,3,2:T(8,128)} %get-tuple-element.360, f32[1,128,2,128]{1,0,3,2:T(1,128)S(1)} %copy.134, s32[]{:T(128)S(6)} %copy.145, s32[]{:T(128)} %constant.31.clone.1..sunk, s32[]{:T(128)} %constant.31.clone.1..sunk, s32[]{:T(128)} %constant.31.clone.1..sunk) | dynamic-update-slice | bytes 262148 | tf_op jit(solution)/shard_map/while/body/jit(dynamic_update_index_in_dim)/dynamic_update_slice | solution.py:136
  143.0 0.9 fusion.154
  144.3 0.9 constant_dynamic-slice_fusion.10
  145.4 0.9 constant_dynamic-slice_fusion.9
  148.6 4.7 %dynamic_update_slice.5 = f32[8,128,2,128]{1,0,3,2:T(8,128)} dynamic-update-slice(f32[8,128,2,128]{1,0,3,2:T(8,128)} %get-tuple-element.360, f32[1,128,2,128]{1,0,3,2:T(1,128)S(1)} %copy.134, s32[]{:T(128)S(6)} %copy.145, s32[]{:T(128)} %constant.31.clone.1..sunk, s32[]{:T(128)} %constant.31.clone.1..sunk, s32[]{:T(128)} %constant.31.clone.1..sunk) | dynamic-update-slice | bytes 262148 | tf_op jit(solution)/shard_map/while/body/jit(dynamic_update_index_in_dim)/dynamic_update_slice | solution.py:136
  157.1 0.9 fusion.154
  158.3 0.9 constant_dynamic-slice_fusion.10
  159.5 0.9 constant_dynamic-slice_fusion.9
  162.6 4.7 %dynamic_update_slice.5 = f32[8,128,2,128]{1,0,3,2:T(8,128)} dynamic-update-slice(f32[8,128,2,128]{1,0,3,2:T(8,128)} %get-tuple-element.360, f32[1,128,2,128]{1,0,3,2:T(1,128)S(1)} %copy.134, s32[]{:T(128)S(6)} %copy.145, s32[]{:T(128)} %constant.31.clone.1..sunk, s32[]{:T(128)} %constant.31.clone.1..sunk, s32[]{:T(128)} %constant.31.clone.1..sunk) | dynamic-update-slice | bytes 262148 | tf_op jit(solution)/shard_map/while/body/jit(dynamic_update_index_in_dim)/dynamic_update_slice | solution.py:136
  171.1 0.9 fusion.154
  172.4 0.9 constant_dynamic-slice_fusion.10
  173.5 0.9 constant_dynamic-slice_fusion.9
  176.6 4.7 %dynamic_update_slice.5 = f32[8,128,2,128]{1,0,3,2:T(8,128)} dynamic-update-slice(f32[8,128,2,128]{1,0,3,2:T(8,128)} %get-tuple-element.360, f32[1,128,2,128]{1,0,3,2:T(1,128)S(1)} %copy.134, s32[]{:T(128)S(6)} %copy.145, s32[]{:T(128)} %constant.31.clone.1..sunk, s32[]{:T(128)} %constant.31.clone.1..sunk, s32[]{:T(128)} %constant.31.clone.1..sunk) | dynamic-update-slice | bytes 262148 | tf_op jit(solution)/shard_map/while/body/jit(dynamic_update_index_in_dim)/dynamic_update_slice | solution.py:136
  185.1 0.9 fusion.154
  186.4 0.9 constant_dynamic-slice_fusion.10
  187.6 0.9 constant_dynamic-slice_fusion.9
  190.7 4.7 %dynamic_update_slice.5 = f32[8,128,2,128]{1,0,3,2:T(8,128)} dynamic-update-slice(f32[8,128,2,128]{1,0,3,2:T(8,128)} %get-tuple-element.360, f32[1,128,2,128]{1,0,3,2:T(1,128)S(1)} %copy.134, s32[]{:T(128)S(6)} %copy.145, s32[]{:T(128)} %constant.31.clone.1..sunk, s32[]{:T(128)} %constant.31.clone.1..sunk, s32[]{:T(128)} %constant.31.clone.1..sunk) | dynamic-update-slice | bytes 262148 | tf_op jit(solution)/shard_map/while/body/jit(dynamic_update_index_in_dim)/dynamic_update_slice | solution.py:136
  199.2 0.9 fusion.154
  200.5 0.9 constant_dynamic-slice_fusion.10
  201.6 0.9 constant_dynamic-slice_fusion.9
  204.7 4.7 %dynamic_update_slice.5 = f32[8,128,2,128]{1,0,3,2:T(8,128)} dynamic-update-slice(f32[8,128,2,128]{1,0,3,2:T(8,128)} %get-tuple-element.360, f32[1,128,2,128]{1,0,3,2:T(1,128)S(1)} %copy.134, s32[]{:T(128)S(6)} %copy.145, s32[]{:T(128)} %constant.31.clone.1..sunk, s32[]{:T(128)} %constant.31.clone.1..sunk, s32[]{:T(128)} %constant.31.clone.1..sunk) | dynamic-update-slice | bytes 262148 | tf_op jit(solution)/shard_map/while/body/jit(dynamic_update_index_in_dim)/dynamic_update_slice | solution.py:136
  210.4 1.6 fusion.31
  212.8 3.7 all-to-all-start
  216.5 6.9 %all-to-all-done = bf16[4,256,256]{1,2,0:T(8,128)(2,1)S(1)} async-done(((bf16[4,256,256]{1,2,0:T(8,128)(2,1)}), bf16[4,256,256]{1,2,0:T(8,128)(2,1)S(1)}, u32[]{:S(2)}, u32[]{:S(2)}) %all-to-all-start) | async-done | bytes 524320 | tf_op jit(solution)/shard_map/all_to_all | solution.py:217
  223.4 3.9 multiply_reduce_fusion
  227.4 1.2 multiply_convert_fusion.1
  228.7 0.8 pad_maximum_fusion
  229.8 52.7 %all-gather.12.cloned.1.call-done = bf16[1024,2048]{1,0:T(8,128)(2,1)} async-done(((bf16[256,2048]{1,0:T(8,128)(2,1)}), bf16[1024,2048]{1,0:T(8,128)(2,1)}) %all-gather.12.cloned.1.call-update) | async-done | bytes 4194320 | tf_op jit(solution)/shard_map/all_gather | solution.py:226
  282.5 77.2 %all-gather.14.cloned.1.call-done = bf16[2048,4224]{1,0:T(8,128)(2,1)} async-done(((bf16[64,4224]{1,0:T(8,128)(2,1)}), bf16[2048,4224]{1,0:T(8,128)(2,1)}) %all-gather.14.cloned.1.call-update) | async-done | bytes 17301520 | tf_op jit(solution)/shard_map/all_gather | solution.py:19
  359.6 11.7 %fusion.21 = f32[1024,1408]{1,0:T(8,128)} fusion(bf16[1024,2048]{1,0:T(8,128)(2,1)} %all-gather.12.cloned.1.call-done, bf16[2048,4224]{1,0:T(8,128)(2,1)} %all-gather.14.cloned.1.call-done), kind=kOutput, calls=%fused_computation.48 | convolution fusion | flops 5905580032 | bytes 15728640 | tf_op jit(solution)/shard_map/dot_general | solution.py:227
  371.3 22.7 %fusion.25 = bf16[1024,2048]{1,0:T(8,128)(2,1)} fusion(bf16[2048,4224]{1,0:T(8,128)(2,1)} %all-gather.14.cloned.1.call-done, f32[1024,1408]{1,0:T(8,128)} %fusion.21, bf16[1024,2048]{1,0:T(8,128)(2,1)} %all-gather.12.cloned.1.call-done), kind=kOutput, calls=%fused_computation.51 | convolution fusion | flops 11821907968 | bytes 25690112 | tf_op jit(solution)/shard_map/dot_general | solution.py:230
  394.0 45.9 %reduce-scatter.2.cloned.1.call-done = bf16[256,2048]{1,0:T(8,128)(2,1)} async-done(((bf16[1024,2048]{1,0:T(8,128)(2,1)}), bf16[256,2048]{1,0:T(8,128)(2,1)}) %reduce-scatter.2.cloned.1.call-update) | async-done | bytes 1048592 | tf_op jit(solution)/shard_map/reduce_scatter | solution.py:231
  439.9 2.5 add_convert_fusion
  (263 shorter events, 54.9 us)
Async XLA Ops:
  6.5 37.1 %copy-start.9 = (u32[128]{0:T(128)S(1)}, u32[128]{0:T(128)}, u32[]{:S(2)}) copy-start(u32[128]{0:T(128)} %constant.104) | copy-start | bytes 1540
  6.5 38.5 %copy-start.1 = (bf16[1024,256]{1,0:T(8,128)(2,1)S(1)}, bf16[1024,256]{1,0:T(8,128)(2,1)}, u32[]{:S(2)}) copy-start(bf16[1024,256]{1,0:T(8,128)(2,1)} %param.17) | copy-start | bytes 1572868
  6.5 216.9 %all-gather.10.cloned.1.call-start = ((), (), s32[]{:S(2)}) async-start(), calls=%async_computation.2 | async-start | bytes 5242880 | tf_op jit(solution)/shard_map/all_gather | solution.py:220
  19.7 54.4 %copy-start = (bf16[1024,256]{1,0:T(8,128)(2,1)S(1)}, bf16[1024,256]{1,0:T(8,128)(2,1)}, u32[]{:S(2)}) copy-start(bf16[1024,256]{1,0:T(8,128)(2,1)} %param.16) | copy-start | bytes 1572868
  30.2 0.5 copy-start.7
  60.6 0.6 copy-start.8
  97.7 112.4 %copy-start.2 = (bf16[1024,256]{1,0:T(8,128)(2,1)S(1)}, bf16[1024,256]{1,0:T(8,128)(2,1)}, u32[]{:S(2)}) copy-start(bf16[1024,256]{1,0:T(8,128)(2,1)} %param.20) | copy-start | bytes 1572868
  210.1 6.4 %copy-start.6 = (bf16[2048]{0:T(1024)(128)(2,1)S(1)}, bf16[2048]{0:T(1024)(128)(2,1)}, u32[]{:S(2)}) copy-start(bf16[2048]{0:T(1024)(128)(2,1)} %param.24) | copy-start | bytes 12292
  212.8 10.7 %all-to-all-start = ((bf16[4,256,256]{1,2,0:T(8,128)(2,1)}), bf16[4,256,256]{1,2,0:T(8,128)(2,1)S(1)}, u32[]{:S(2)}, u32[]{:S(2)}) async-start(bf16[4,256,256]{1,2,0:T(8,128)(2,1)} %bitcast.516), calls=%async_computation | async-start | bytes 1048576 | tf_op jit(solution)/shard_map/all_to_all | solution.py:217
  216.5 66.0 %all-gather.12.cloned.1.call-start = ((), (), s32[]{:S(2)}) async-start(), calls=%async_computation.3 | async-start | bytes 5242880 | tf_op jit(solution)/shard_map/all_gather | solution.py:226
  227.3 1.3 copy-start.3
  227.3 1.3 copy-start.4
  227.3 1.3 copy-start.5
  228.6 131.1 %all-gather.14.cloned.1.call-start = ((), (), s32[]{:S(2)}) async-start(), calls=%async_computation.4 | async-start | bytes 17842176 | tf_op jit(solution)/shard_map/all_gather | solution.py:19
  229.5 210.4 %reduce-scatter.2.cloned.1.call-start = ((), (), s32[]{:S(2)}) async-start(), calls=%async_computation.5 | async-start | bytes 5242880 | tf_op jit(solution)/shard_map/reduce_scatter | solution.py:231
Sparse Core Ops, SparseCore 0:
  9.0 51.1 all-gather.9
  228.7 53.7 all-gather.11
  284.7 74.8 all-gather.13
  394.2 45.7 reduce-scatter.1
where the time goes:
time: 451 us; the launch traced here: 449 us
  waiting for transfers between devices  183 us (41%)
  local copies, waits for them, and re-layouts  78.3 us (17%)
  matrix products  58.1 us (13%)
  blocking collectives  42.2 us (9%)
  other arithmetic  39.2 us (9%)
  between operations  32.8 us (7%)
  loops' own time  10.8 us (2%)
    all_gather x1, waiting for transfers between devices, gather_turned(): lax.all_gather(both, axis, axis=0, tiled=True)  77.2 us
    all_gather x1, waiting for transfers between devices, body(): rows_all = lax.all_gather(normed, 'tp', axis=0, tiled=True)  52.7 us
    reduce_scatter x1, waiting for transfers between devices, body(): lax.psum_scatter(partial_sum.astype(jnp.bfloat16), 'tp', scatter_dimensio...  45.9 us
    dynamic_update_slice x16, local copies, waits for them, and re-layouts, run_blocks(): final, outputs = lax.scan(block_step, start_state, inputs)  38.7 us
    all_gather x3, blocking collectives, all_in_one(): both, at, found = (lax.all_gather(jnp.concatenate(lines), axis), 0, {})  26.6 us
    dot_general x1, matrix products, body(): jnp.dot(hidden, whole_down, preferred_element_type=jnp.float32)  22.7 us
    unnamed x3, blocking collectives  15.6 us
    dynamic_slice x16, local copies, waits for them, and re-layouts, run_blocks(): final, outputs = lax.scan(block_step, start_state, inputs)  14.8 us
  transfers between devices with their start and end apart: 5, of which 4 were waited for; matrix products, arithmetic and copies ran while one was open for 30% of the time, Pallas kernels for 0%

commit v1 on v0

--- a/solution.py
+++ b/solution.py
@@ -223,7 +223,9 @@
     stream = residual.astype(jnp.float32) + projected
     normed = stream * lax.rsqrt(jnp.mean(stream * stream, axis=1, keepdims=True) + norm_eps)
     normed = (normed * norm_gain.astype(jnp.float32)).astype(jnp.bfloat16)
-    rows_all = lax.all_gather(normed, "tp", axis=0, tiled=True)
+    rows_all = jnp.concatenate(
+        lax.all_to_all(jnp.stack([normed] * lax.axis_size("tp")), "tp", 0, 0), axis=0
+    )
     gate_act = jnp.dot(rows_all, whole_gate, preferred_element_type=jnp.float32)
     up_act = jnp.dot(rows_all, whole_up, preferred_element_type=jnp.float32)
     hidden = (jax.nn.silu(gate_act) * up_act).astype(jnp.bfloat16)

time: 451 us -> 372 us (0.82)
  waiting for transfers between devices: 183 us -> 60.4 us
  blocking collectives: 42.2 us -> 85.8 us
    all_gather x1, waiting for transfers between devices: 77.2 us -> 0.01 us  [gather_turned(): lax.all_gather(both, axis, axis=0, tiled=True)]
    all_gather x1 -> x0, waiting for transfers between devices: 52.7 us -> none  [body(): rows_all = lax.all_gather(normed, 'tp', axis=0, tiled=True)]
    all_to_all x0 -> x1, blocking collectives: none -> 43.1 us  [body(): lax.all_to_all(jnp.stack([normed] * lax.axis_size('tp')), 'tp', 0, 0)]
    reduce_scatter x1, waiting for transfers between devices: 45.9 us -> 52.8 us  [body(): lax.psum_scatter(partial_sum.astype(jnp.bfloat16), 'tp', scatter_dimensio...]
  transfers between devices with their start and end apart: 5 -> 4, of which waited for: 4 -> 2; matrix products, arithmetic and copies ran while one was open for 30% -> 38% of each run, Pallas kernels for 0% -> 0%
where the time goes in v1:
time: 372 us; the launch traced here: 369 us
  blocking collectives  85.8 us (23%)
  local copies, waits for them, and re-layouts  79.2 us (21%)
  waiting for transfers between devices  60.4 us (16%)
  matrix products  56 us (15%)
  other arithmetic  40.4 us (11%)
  between operations  32.5 us (9%)
  loops' own time  11 us (3%)
  starting transfers between devices  3.77 us (1%)
    reduce_scatter x1, waiting for transfers between devices, body(): lax.psum_scatter(partial_sum.astype(jnp.bfloat16), 'tp', scatter_dimensio...  52.8 us
    all_to_all x1, blocking collectives, body(): lax.all_to_all(jnp.stack([normed] * lax.axis_size('tp')), 'tp', 0, 0)  43.1 us
    dynamic_update_slice x16, local copies, waits for them, and re-layouts, run_blocks(): final, outputs = lax.scan(block_step, start_state, inputs)  38.8 us
    all_gather x3, blocking collectives, all_in_one(): both, at, found = (lax.all_gather(jnp.concatenate(lines), axis), 0, {})  26.5 us
    dot_general x1, matrix products, body(): jnp.dot(hidden, whole_down, preferred_element_type=jnp.float32)  22.6 us
    unnamed x3, blocking collectives  16.2 us
    dynamic_slice x16, local copies, waits for them, and re-layouts, run_blocks(): final, outputs = lax.scan(block_step, start_state, inputs)  14.9 us
    dot_general x1, matrix products, body(): gate_act = jnp.dot(rows_all, whole_gate, preferred_element_type=jnp.float32)  11.7 us
  transfers between devices with their start and end apart: 4, of which 2 were waited for; matrix products, arithmetic and copies ran while one was open for 38% of the time, Pallas kernels for 0%

profile of v1, /device:TPU:1, one launch (start us, length us, event | category | flops | bytes accessed | tf_op | source)
XLA Modules:
  0.0 369.1 jit_solution(16203192262797785684)
XLA Ops:
  7.3 1.9 pad_maximum_fusion
  10.8 1.2 dynamic-slice
  12.0 2.0 slice_dynamic-update-slice_fusion
  14.0 1.3 broadcast_compare_fusion
  16.5 0.9 fusion.108
  17.5 1.2 copy.56
  19.8 3.0 all-gather.3
  23.5 1.8 all-reduce.6
  30.1 11.8 %all-gather.4 = f32[4,260,128]{2,1,0:T(8,128)S(1)} all-gather(f32[1,260,128]{2,1,0:T(8,128)S(1)} %maximum_bitcast_fusion.1), channel_id=3, replica_groups=mesh['sp_0'=4,'sp_1'=4,'sp_2'=2,'tp'=4] {'sp_1'}, dimensions={0}, use_global_device_ids=true | all-gather | bytes 665600 | tf_op jit(solution)/shard_map/all_gather | solution.py:41
  41.9 0.8 fusion.113
  43.3 0.8 dynamic-update-slice.1
  44.6 6.5 %all-reduce.7 = s32[4]{0:T(128)S(1)} all-reduce(s32[4]{0:T(128)S(1)} %dynamic-update-slice.1), channel_id=1, replica_groups=mesh['sp_0'=4,'sp_1'=4,'sp_2'=2,'tp'=4] {'sp_1'}, use_global_device_ids=true, to_apply=%add.7 | all-reduce | flops 4 | bytes 32
  59.9 11.7 %all-gather.5 = f32[4,260,128]{2,1,0:T(8,128)S(1)} all-gather(f32[1,260,128]{2,1,0:T(8,128)S(1)} %maximum_bitcast_fusion.2), channel_id=4, replica_groups=mesh['sp_0'=4,'sp_1'=4,'sp_2'=2,'tp'=4] {'sp_0'}, dimensions={0}, use_global_device_ids=true | all-gather | bytes 665600 | tf_op jit(solution)/shard_map/all_gather | solution.py:41
  71.6 0.9 fusion.111
  72.5 1.5 reshape.2050
  75.4 7.8 %all-reduce.8 = s32[4]{0:T(128)S(1)} all-reduce(s32[4]{0:T(128)S(1)} %dynamic-update-slice.2), channel_id=1, replica_groups=mesh['sp_0'=4,'sp_1'=4,'sp_2'=2,'tp'=4] {'sp_0'}, use_global_device_ids=true, to_apply=%add.8 | all-reduce | flops 4 | bytes 32
  91.5 2.0 copy.45
  93.5 1.1 convert_multiply_fusion
  94.7 1.5 reshape.2052
  96.3 0.9 add_select_fusion.5
  97.2 2.0 add_select_fusion.3
  99.3 112.8 %while.18 = (s32[]{:T(128)}, f32[2,128,128]{2,1,0:T(8,128)S(1)}, f32[2,128]{1,0:T(2,128)S(1)}, f32[2]{0:T(128)S(1)}, s32[]{:T(128)}, /*index=5*/f32[8,128,2,128]...) while((s32[]{:T(128)}, f32[2,128,128]{2,1,0:T(8,128)S(1)}, ...), condition=%wide.region_8.9_spmd, body=%wide.region_3.8_spmd.sunk | while | flops 202756624 | bytes 3499011 | solution.py:136
  102.4 0.9 fusion.154
  103.7 0.9 constant_dynamic-slice_fusion.10
  104.9 0.9 constant_dynamic-slice_fusion.9
  108.0 4.8 %dynamic_update_slice.5 = f32[8,128,2,128]{1,0,3,2:T(8,128)} dynamic-update-slice(f32[8,128,2,128]{1,0,3,2:T(8,128)} %get-tuple-element.360, f32[1,128,2,128]{1,0,3,2:T(1,128)S(1)} %copy.134, s32[]{:T(128)S(6)} %copy.145, s32[]{:T(128)} %constant.31.clone.1..sunk, s32[]{:T(128)} %constant.31.clone.1..sunk, s32[]{:T(128)} %constant.31.clone.1..sunk) | dynamic-update-slice | bytes 262148 | tf_op jit(solution)/shard_map/while/body/jit(dynamic_update_index_in_dim)/dynamic_update_slice | solution.py:136
  116.5 0.9 fusion.154
  117.8 1.0 constant_dynamic-slice_fusion.10
  119.0 0.9 constant_dynamic-slice_fusion.9
  122.1 4.8 %dynamic_update_slice.5 = f32[8,128,2,128]{1,0,3,2:T(8,128)} dynamic-update-slice(f32[8,128,2,128]{1,0,3,2:T(8,128)} %get-tuple-element.360, f32[1,128,2,128]{1,0,3,2:T(1,128)S(1)} %copy.134, s32[]{:T(128)S(6)} %copy.145, s32[]{:T(128)} %constant.31.clone.1..sunk, s32[]{:T(128)} %constant.31.clone.1..sunk, s32[]{:T(128)} %constant.31.clone.1..sunk) | dynamic-update-slice | bytes 262148 | tf_op jit(solution)/shard_map/while/body/jit(dynamic_update_index_in_dim)/dynamic_update_slice | solution.py:136
  130.7 0.9 fusion.154
  132.0 0.9 constant_dynamic-slice_fusion.10
  133.1 0.9 constant_dynamic-slice_fusion.9
  136.2 4.7 %dynamic_update_slice.5 = f32[8,128,2,128]{1,0,3,2:T(8,128)} dynamic-update-slice(f32[8,128,2,128]{1,0,3,2:T(8,128)} %get-tuple-element.360, f32[1,128,2,128]{1,0,3,2:T(1,128)S(1)} %copy.134, s32[]{:T(128)S(6)} %copy.145, s32[]{:T(128)} %constant.31.clone.1..sunk, s32[]{:T(128)} %constant.31.clone.1..sunk, s32[]{:T(128)} %constant.31.clone.1..sunk) | dynamic-update-slice | bytes 262148 | tf_op jit(solution)/shard_map/while/body/jit(dynamic_update_index_in_dim)/dynamic_update_slice | solution.py:136
  144.8 0.9 fusion.154
  146.1 0.9 constant_dynamic-slice_fusion.10
  147.2 0.9 constant_dynamic-slice_fusion.9
  150.3 4.7 %dynamic_update_slice.5 = f32[8,128,2,128]{1,0,3,2:T(8,128)} dynamic-update-slice(f32[8,128,2,128]{1,0,3,2:T(8,128)} %get-tuple-element.360, f32[1,128,2,128]{1,0,3,2:T(1,128)S(1)} %copy.134, s32[]{:T(128)S(6)} %copy.145, s32[]{:T(128)} %constant.31.clone.1..sunk, s32[]{:T(128)} %constant.31.clone.1..sunk, s32[]{:T(128)} %constant.31.clone.1..sunk) | dynamic-update-slice | bytes 262148 | tf_op jit(solution)/shard_map/while/body/jit(dynamic_update_index_in_dim)/dynamic_update_slice | solution.py:136
  158.9 0.9 fusion.154
  160.2 0.9 constant_dynamic-slice_fusion.10
  161.3 0.9 constant_dynamic-slice_fusion.9
  164.4 4.7 %dynamic_update_slice.5 = f32[8,128,2,128]{1,0,3,2:T(8,128)} dynamic-update-slice(f32[8,128,2,128]{1,0,3,2:T(8,128)} %get-tuple-element.360, f32[1,128,2,128]{1,0,3,2:T(1,128)S(1)} %copy.134, s32[]{:T(128)S(6)} %copy.145, s32[]{:T(128)} %constant.31.clone.1..sunk, s32[]{:T(128)} %constant.31.clone.1..sunk, s32[]{:T(128)} %constant.31.clone.1..sunk) | dynamic-update-slice | bytes 262148 | tf_op jit(solution)/shard_map/while/body/jit(dynamic_update_index_in_dim)/dynamic_update_slice | solution.py:136
  173.0 0.9 fusion.154
  174.3 0.9 constant_dynamic-slice_fusion.10
  175.4 0.9 constant_dynamic-slice_fusion.9
  178.5 4.7 %dynamic_update_slice.5 = f32[8,128,2,128]{1,0,3,2:T(8,128)} dynamic-update-slice(f32[8,128,2,128]{1,0,3,2:T(8,128)} %get-tuple-element.360, f32[1,128,2,128]{1,0,3,2:T(1,128)S(1)} %copy.134, s32[]{:T(128)S(6)} %copy.145, s32[]{:T(128)} %constant.31.clone.1..sunk, s32[]{:T(128)} %constant.31.clone.1..sunk, s32[]{:T(128)} %constant.31.clone.1..sunk) | dynamic-update-slice | bytes 262148 | tf_op jit(solution)/shard_map/while/body/jit(dynamic_update_index_in_dim)/dynamic_update_slice | solution.py:136
  187.1 0.9 fusion.154
  188.3 0.9 constant_dynamic-slice_fusion.10
  189.5 0.9 constant_dynamic-slice_fusion.9
  192.6 4.7 %dynamic_update_slice.5 = f32[8,128,2,128]{1,0,3,2:T(8,128)} dynamic-update-slice(f32[8,128,2,128]{1,0,3,2:T(8,128)} %get-tuple-element.360, f32[1,128,2,128]{1,0,3,2:T(1,128)S(1)} %copy.134, s32[]{:T(128)S(6)} %copy.145, s32[]{:T(128)} %constant.31.clone.1..sunk, s32[]{:T(128)} %constant.31.clone.1..sunk, s32[]{:T(128)} %constant.31.clone.1..sunk) | dynamic-update-slice | bytes 262148 | tf_op jit(solution)/shard_map/while/body/jit(dynamic_update_index_in_dim)/dynamic_update_slice | solution.py:136
  201.2 0.9 fusion.154
  202.4 0.9 constant_dynamic-slice_fusion.10
  203.6 0.9 constant_dynamic-slice_fusion.9
  206.7 4.7 %dynamic_update_slice.5 = f32[8,128,2,128]{1,0,3,2:T(8,128)} dynamic-update-slice(f32[8,128,2,128]{1,0,3,2:T(8,128)} %get-tuple-element.360, f32[1,128,2,128]{1,0,3,2:T(1,128)S(1)} %copy.134, s32[]{:T(128)S(6)} %copy.145, s32[]{:T(128)} %constant.31.clone.1..sunk, s32[]{:T(128)} %constant.31.clone.1..sunk, s32[]{:T(128)} %constant.31.clone.1..sunk) | dynamic-update-slice | bytes 262148 | tf_op jit(solution)/shard_map/while/body/jit(dynamic_update_index_in_dim)/dynamic_update_slice | solution.py:136
  212.1 1.6 fusion.31
  213.7 0.8 copy.115
  214.6 3.7 %all-to-all-start = ((bf16[4,256,256]{1,2,0:T(8,128)(2,1)}), bf16[4,256,256]{1,2,0:T(8,128)(2,1)S(1)}, u32[]{:S(2)}, u32[]{:S(2)}) async-start(bf16[4,256,256]{1,2,0:T(8,128)(2,1)} %bitcast.517), calls=%async_computation | async-start | bytes 1048576 | tf_op jit(solution)/shard_map/all_to_all | solution.py:217
  218.3 6.9 %all-to-all-done = bf16[4,256,256]{1,2,0:T(8,128)(2,1)S(1)} async-done(((bf16[4,256,256]{1,2,0:T(8,128)(2,1)}), bf16[4,256,256]{1,2,0:T(8,128)(2,1)S(1)}, u32[]{:S(2)}, u32[]{:S(2)}) %all-to-all-start) | async-done | bytes 524320 | tf_op jit(solution)/shard_map/all_to_all | solution.py:217
  225.2 3.9 %multiply_reduce_fusion = (f32[256]{0:T(256)S(1)}, f32[256,2048]{1,0:T(8,128)S(1)}) fusion(bf16[256,1024]{0,1:T(8,128)(2,1)S(1)} %bitcast.575, bf16[1024,2048]{1,0:T(8,128)(2,1)} %all-gather.9.cloned.1.call-done, bf16[256,2048]{1,0:T(8,128)(2,1)} %param.22), kind=kOutput, calls=%fused_computation.56 | convolution fusion | flops 1075838720 | bytes 7865344 | tf_op jit(solution)/shard_map/dot_general | solution.py:218
  229.9 43.1 %all_to_all.24 = bf16[4,256,2048]{2,1,0:T(8,128)(2,1)} all-to-all(bf16[4,256,2048]{2,1,0:T(8,128)(2,1)S(1)} %stack.2), channel_id=1, replica_groups=mesh['sp_0'=4,'sp_1'=4,'sp_2'=2,'tp'=4] {'tp'}, dimensions={0} | all-to-all | bytes 8388608 | tf_op jit(solution)/shard_map/all_to_all | solution.py:227
  273.0 11.7 %fusion.21 = f32[1024,1408]{1,0:T(8,128)} fusion(bf16[1024,2048]{1,0:T(8,128)(2,1)} %bitcast.572, bf16[2048,4224]{1,0:T(8,128)(2,1)} %all-gather.11.cloned.1.call-done), kind=kOutput, calls=%fused_computation.48 | convolution fusion | flops 5905580032 | bytes 15728640 | tf_op jit(solution)/shard_map/dot_general | solution.py:229
  284.6 22.6 %fusion.25 = bf16[1024,2048]{1,0:T(8,128)(2,1)} fusion(bf16[2048,4224]{1,0:T(8,128)(2,1)} %all-gather.11.cloned.1.call-done, f32[1024,1408]{1,0:T(8,128)} %fusion.21, bf16[1024,2048]{1,0:T(8,128)(2,1)} %bitcast.573), kind=kOutput, calls=%fused_computation.51 | convolution fusion | flops 11821907968 | bytes 25690112 | tf_op jit(solution)/shard_map/dot_general | solution.py:232
  307.3 52.8 %reduce-scatter.2.cloned.1.call-done = bf16[256,2048]{1,0:T(8,128)(2,1)} async-done(((bf16[1024,2048]{1,0:T(8,128)(2,1)}), bf16[256,2048]{1,0:T(8,128)(2,1)}) %reduce-scatter.2.cloned.1.call-update) | async-done | bytes 1048592 | tf_op jit(solution)/shard_map/reduce_scatter | solution.py:233
  360.1 2.5 add_convert_fusion
  (262 shorter events, 53.3 us)
Async XLA Ops:
  6.5 12.2 %copy-start = (bf16[1024,256]{1,0:T(8,128)(2,1)S(1)}, bf16[1024,256]{1,0:T(8,128)(2,1)}, u32[]{:S(2)}) copy-start(bf16[1024,256]{1,0:T(8,128)(2,1)} %param.16) | copy-start | bytes 1572868
  6.5 12.5 %copy-start.2 = (bf16[1024,256]{1,0:T(8,128)(2,1)S(1)}, bf16[1024,256]{1,0:T(8,128)(2,1)}, u32[]{:S(2)}) copy-start(bf16[1024,256]{1,0:T(8,128)(2,1)} %param.17) | copy-start | bytes 1572868
  6.5 218.7 %all-gather.9.cloned.1.call-start = ((), (), s32[]{:S(2)}) async-start(), calls=%async_computation.3 | async-start | bytes 5242880 | tf_op jit(solution)/shard_map/all_gather | solution.py:220
  7.3 265.7 %all-gather.11.cloned.1.call-start = ((), (), s32[]{:S(2)}) async-start(), calls=%async_computation.4 | async-start | bytes 17842176 | tf_op jit(solution)/shard_map/all_gather | solution.py:19
  9.2 33.5 %copy-start.9 = (u32[128]{0:T(128)S(1)}, u32[128]{0:T(128)}, u32[]{:S(2)}) copy-start(u32[128]{0:T(128)} %constant.104) | copy-start | bytes 1540
  29.9 44.1 %copy-start.8 = (u32[128]{0:T(128)S(1)}, u32[128]{0:T(128)}, u32[]{:S(2)}) copy-start(u32[128]{0:T(128)} %constant.109) | copy-start | bytes 1540
  71.6 19.9 %copy-start.1 = (f32[4,260,128]{2,1,0:T(8,128)}, f32[4,260,128]{2,1,0:T(8,128)S(1)}, u32[]{:S(2)}) copy-start(f32[4,260,128]{2,1,0:T(8,128)S(1)} %all-gather.5) | copy-start | bytes 1597444
  74.0 23.2 %copy-start.4 = (f32[1,256,128]{2,1,0:T(8,128)S(1)}, f32[1,256,128]{2,1,0:T(8,128)}, u32[]{:S(2)}) copy-start(f32[1,256,128]{2,1,0:T(8,128)} %get-tuple-element.171) | copy-start | bytes 393220
  74.0 23.2 %copy-start.5 = (f32[1,256,128]{2,1,0:T(8,128)S(1)}, f32[1,256,128]{2,1,0:T(8,128)}, u32[]{:S(2)}) copy-start(f32[1,256,128]{2,1,0:T(8,128)} %get-tuple-element.172) | copy-start | bytes 393220
  74.0 23.2 %copy-start.6 = (f32[1,256,128]{2,1,0:T(8,128)S(1)}, f32[1,256,128]{2,1,0:T(8,128)}, u32[]{:S(2)}) copy-start(f32[1,256,128]{2,1,0:T(8,128)} %get-tuple-element.173) | copy-start | bytes 393220
  99.3 112.9 %copy-start.3 = (bf16[1024,256]{0,1:T(8,128)(2,1)S(1)}, bf16[1024,256]{0,1:T(8,128)(2,1)}, u32[]{:S(2)}) copy-start(bf16[1024,256]{0,1:T(8,128)(2,1)} %copy.45) | copy-start | bytes 1572868
  212.1 6.2 %copy-start.7 = (bf16[2048]{0:T(1024)(128)(2,1)S(1)}, bf16[2048]{0:T(1024)(128)(2,1)}, u32[]{:S(2)}) copy-start(bf16[2048]{0:T(1024)(128)(2,1)} %param.24) | copy-start | bytes 12292
  214.6 10.7 %all-to-all-start = ((bf16[4,256,256]{1,2,0:T(8,128)(2,1)}), bf16[4,256,256]{1,2,0:T(8,128)(2,1)S(1)}, u32[]{:S(2)}, u32[]{:S(2)}) async-start(bf16[4,256,256]{1,2,0:T(8,128)(2,1)} %bitcast.517), calls=%async_computation | async-start | bytes 1048576 | tf_op jit(solution)/shard_map/all_to_all | solution.py:217
  218.3 141.8 %reduce-scatter.2.cloned.1.call-start = ((), (), s32[]{:S(2)}) async-start(), calls=%async_computation.5 | async-start | bytes 5242880 | tf_op jit(solution)/shard_map/reduce_scatter | solution.py:233
Sparse Core Ops, SparseCore 0:
  9.0 51.1 all-gather.8
  62.4 74.9 all-gather.10
  307.4 52.5 reduce-scatter.1
